TPU v7x, 128 devices: a whole 4x4x4 slice. The times are simulated.
128 devices in a mesh: sp: 32 (over z, y, core), tp: 4 (over x).
Axes of the slice: x: 4, y: 4, z: 4, core: 2. Of those that a mesh axis runs over, the one named last changes fastest.
Arguments:
- tokens: bfloat16 [12288, 2048], P(('sp', 'tp')), may hold values from -8 to 8, as said below
- query_weight: bfloat16 [2048, 1024], P(None, 'tp'), as said below
- key_weight: bfloat16 [2048, 256], P(None, 'tp'), as said below
- value_weight: bfloat16 [2048, 256], P(None, 'tp'), may hold values from -0.125 to 0.125
- out_weight: bfloat16 [1024, 2048], P('tp'), may hold values from -0.75 to 0.75
- query_gain: bfloat16 [16, 64], P('tp'), may hold values from 0.5 to 6.5
- key_gain: bfloat16 [4, 64], P('tp'), may hold values from 0.5 to 6.5
Outputs:
- mixed: bfloat16 [12288, 2048], P(('sp', 'tp'))
- log_sums: float32 [16, 12288], P('tp', 'sp')
Inputs may be any that keep to these rules, and one draw needn't show every extreme that they name: Each block of 384 consecutive tokens has a mean vector of its own. `query_weight`: entries are those of a weight over 2048 inputs, of magnitude at most 6 / sqrt(2048). `key_weight`: entries are those of a weight over 2048 inputs, of magnitude at most 6 / sqrt(2048).
All inputs are finite; a program needn't handle non-finite values.
Results may differ from a plain program's by a relative error of at most 0.028.
Values may be sent and summed in bfloat16 or wider, within the bound.
A program may use at most 64 MiB of HBM per device.

v0:
```python
import math
import jax
import jax.numpy as jnp
from jax import lax
from jax.sharding import PartitionSpec as P

GRID_W = 64
ROPE_BASE = 10000.0


def in_order(tiles, dim):
    dims = list(tiles.shape[1:])
    dims[dim] *= tiles.shape[0]
    return jnp.moveaxis(tiles, 0, dim).reshape(dims)


def copy_for_each(array, axis):
    count = lax.axis_size(axis)
    return lax.all_to_all(
        jnp.broadcast_to(array[None], (count, *array.shape)), axis, 0, 0, tiled=True
    )


def collect(array, axis, dim):
    return in_order(copy_for_each(array, axis), dim)


def side_by_side(arrays, axis, dim, along):
    widths = [a.shape[along] for a in arrays]
    both = jnp.concatenate(arrays, axis=along)
    out = lax.all_gather(both, axis, axis=dim, tiled=True)
    return tuple(jnp.split(out, [sum(widths[:k]) for k in range(1, len(widths))], axis=along))


def angle_tables(first, count, quarter):
    place = first + jnp.arange(count, dtype=jnp.int32)
    grid_row = (place // GRID_W).astype(jnp.float32)
    grid_col = (place % GRID_W).astype(jnp.float32)
    freq = ROPE_BASE ** (-jnp.arange(quarter, dtype=jnp.float32) / quarter)
    row_angle = grid_row[:, None] * freq[None, :]
    col_angle = grid_col[:, None] * freq[None, :]
    return (jnp.cos(row_angle), jnp.sin(row_angle), jnp.cos(col_angle), jnp.sin(col_angle))


def turn_pairs(part, cosine, sine):
    quarter = part.shape[-1] // 2
    first = part[..., :quarter]
    second = part[..., quarter:]
    cosine = cosine[:, None, :]
    sine = sine[:, None, :]
    return jnp.concatenate(
        [first * cosine - second * sine, second * cosine + first * sine], axis=-1
    )


def prepare(raw, gain, first):
    count = raw.shape[0]
    heads, width = gain.shape
    values = raw.astype(jnp.float32).reshape(count, heads, width)
    scaled = values * lax.rsqrt(jnp.mean(values * values, axis=-1, keepdims=True) + 1e-06)
    scaled = scaled * gain.astype(jnp.float32)[None, :, :]
    row_cos, row_sin, col_cos, col_sin = angle_tables(first, count, width // 4)
    half = width // 2
    turned = jnp.concatenate(
        [
            turn_pairs(scaled[..., :half], row_cos, row_sin),
            turn_pairs(scaled[..., half:], col_cos, col_sin),
        ],
        axis=-1,
    )
    return turned.astype(jnp.bfloat16)


def group_queries(queries, kv_count):
    count, heads, width = queries.shape
    share = heads // kv_count
    grouped = queries.reshape(count, kv_count, share, width).transpose(1, 0, 2, 3)
    return grouped.reshape(kv_count, count * share, width)


def start_state(kv_count, query_rows, width):
    top = jnp.full((kv_count, query_rows), -1e30, jnp.float32)
    total = jnp.zeros((kv_count, query_rows), jnp.float32)
    summed = jnp.zeros((kv_count, query_rows, width), jnp.float32)
    return (top, total, summed)


def fold_keys(state, pieces, grouped, scale):
    keys, values = pieces
    count, kv_count, width = keys.shape
    block_len = math.gcd(count, 1024)
    key_blocks = keys.reshape(count // block_len, block_len, kv_count, width)
    value_blocks = values.reshape(count // block_len, block_len, kv_count, width)

    def inner(carry, block):
        top, total, summed = carry
        key_block, value_block = block
        scores = (
            lax.dot_general(
                grouped, key_block, (((2,), (2,)), ((0,), (1,))), preferred_element_type=jnp.float32
            )
            * scale
        )
        new_top = jnp.maximum(top, jnp.max(scores, axis=-1))
        factor = jnp.exp(top - new_top)
        expo = jnp.exp(scores - new_top[..., None])
        total = total * factor + jnp.sum(expo, axis=-1)
        mixed = lax.dot_general(
            expo.astype(jnp.bfloat16),
            value_block,
            (((2,), (0,)), ((0,), (1,))),
            preferred_element_type=jnp.float32,
        )
        summed = summed * factor[..., None] + mixed
        return ((new_top, total, summed), None)

    state, _ = lax.scan(inner, state, (key_blocks, value_blocks))
    return state


def finish(state, count, share):
    top, total, summed = state
    kv_count, query_rows, width = summed.shape
    attended = (summed / total[..., None]).astype(jnp.bfloat16)
    attended = attended.reshape(kv_count, count, share, width).transpose(1, 0, 2, 3)
    attended = attended.reshape(count, kv_count * share * width)
    log_rows = (top + jnp.log(total)).reshape(kv_count, count, share).transpose(0, 2, 1)
    return (attended, log_rows.reshape(kv_count * share, count))


def body(tokens, query_weight, key_weight, value_weight, out_weight, query_gain, key_gain):
    width = query_gain.shape[1]
    scale = width ** (-0.5)
    query_cols = query_weight.shape[1]
    key_cols = key_weight.shape[1]
    kv_count = key_gain.shape[0]
    share = query_gain.shape[0] // kv_count
    piece = collect(tokens, "tp", 0)
    made = [
        jnp.dot(piece, weight, preferred_element_type=jnp.float32).astype(jnp.bfloat16)
        for weight in (query_weight, key_weight, value_weight)
    ]
    joined = jnp.concatenate(made, axis=1)
    count = joined.shape[0]
    first = lax.axis_index("sp") * count
    queries = prepare(joined[:, :query_cols], query_gain, first)
    keys = prepare(joined[:, query_cols : query_cols + key_cols], key_gain, first)
    values = joined[:, query_cols + key_cols :].reshape(count, kv_count, width)
    grouped = group_queries(queries, kv_count)
    state = fold_keys(
        start_state(kv_count, count * share, width),
        side_by_side((keys, values), "sp", 0, 1),
        grouped=grouped,
        scale=scale,
    )
    attended, log_sums = finish(state, count, share)
    mixed = lax.psum_scatter(
        jnp.dot(attended, out_weight, preferred_element_type=jnp.float32).astype(jnp.bfloat16),
        "tp",
        scatter_dimension=0,
        tiled=True,
    )
    return (mixed, log_sums)


def solution(mesh):
    return jax.shard_map(
        body,
        mesh=mesh,
        in_specs=(
            P(("sp", "tp"), None),
            P(None, "tp"),
            P(None, "tp"),
            P(None, "tp"),
            P("tp", None),
            P("tp", None),
            P("tp", None),
        ),
        out_specs=(P(("sp", "tp"), None), P("tp", "sp")),
        check_vma=False,
    )
```

profile of v0, /device:TPU:0, one launch (start us, length us, event | category | flops | bytes accessed | tf_op | source)
XLA Modules:
  0.0 175.0 jit_solution(1470406230783409071)
XLA Ops:
  7.2 2.4 %broadcast_in_dim.11 = bf16[4,96,2048]{2,1,0:T(8,128)(2,1)} broadcast(bf16[96,2048]{1,0:T(8,128)(2,1)} %param.9), dimensions={1,2} | broadcast | bytes 1966080 | tf_op jit(solution)/shard_map/broadcast_in_dim | solution.py:20
  9.6 4.5 %all-to-all-start = ((bf16[4,96,2048]{2,1,0:T(8,128)(2,1)}), bf16[4,96,2048]{2,1,0:T(8,128)(2,1)S(1)}, u32[]{:S(2)}, u32[]{:S(2)}) async-start(bf16[4,96,2048]{2,1,0:T(8,128)(2,1)} %broadcast_in_dim.11), calls=%async_computation | async-start | bytes 3145728 | tf_op jit(solution)/shard_map/all_to_all | solution.py:19
  14.2 20.7 %all-to-all-done = bf16[4,96,2048]{2,1,0:T(8,128)(2,1)S(1)} async-done(((bf16[4,96,2048]{2,1,0:T(8,128)(2,1)}), bf16[4,96,2048]{2,1,0:T(8,128)(2,1)S(1)}, u32[]{:S(2)}, u32[]{:S(2)}) %all-to-all-start) | async-done | bytes 1572896 | tf_op jit(solution)/shard_map/all_to_all | solution.py:19
  37.5 2.0 %fusion.24 = (f32[384,4]{0,1:T(4,128)S(1)}, bf16[384,256]{0,1:T(8,128)(2,1)S(1)}) fusion(bf16[384,2048]{1,0:T(8,128)(2,1)S(1)} %bitcast.62, bf16[2048,256]{1,0:T(8,128)(2,1)} %param.10), kind=kOutput, calls=%fused_computation.34 | convolution fusion | flops 403044864 | bytes 2824192 | tf_op jit(solution)/shard_map/dot_general | solution.py:140
  41.2 43.2 %all-gather.2.cloned.1.call-done = bf16[12288,2,64]{0,2,1:T(8,128)(2,1)} async-done(((bf16[384,2,64]{0,2,1:T(8,128)(2,1)}), bf16[12288,2,64]{0,2,1:T(8,128)(2,1)}) %all-gather.2.cloned.1.call-update) | async-done | bytes 3145744 | tf_op jit(solution)/shard_map/all_gather | solution.py:31
  84.4 2.2 %fusion.47 = (bf16[12288,1,64]{0,2,1:T(8,128)(2,1)S(1)}, bf16[12288,1,64]{0,2,1:T(8,128)(2,1)S(1)}) fusion(bf16[12288,2,64]{0,2,1:T(8,128)(2,1)} %all-gather.2.cloned.1.call-done), kind=kLoop, calls=%fused_computation.86 | loop fusion | bytes 6291456 | tf_op jit(solution)/shard_map/split | solution.py:32
  86.7 1.3 copy.27
  88.0 52.6 %while.15 = (s32[]{:T(128)}, f32[1,1536]{1,0:T(1,128)S(1)}, f32[1,1536]{1,0:T(1,128)S(1)}, f32[1,1536,64]{1,2,0:T(8,128)S(1)}, bf16[12,1024,1,64]{1,3,2,0:T(8,12...) while((s32[]{:T(128)}, f32[1,1536]{1,0:T(1,128)S(1)}, ...), condition=%wide.region_5.6_spmd.clone, body=%wide.region_2.5_spmd.clone.sunk | while | flops 415540224 | bytes 20420728 | solution.py:117
  89.1 1.1 fusion.65
  90.2 2.2 %fusion.67 = f32[1,1536,64]{1,2,0:T(8,128)S(1)} fusion(f32[1024,1536]{1,0:T(8,128)S(1)} %get-tuple-element.181, f32[1536]{0:T(1024)S(1)} %get-tuple-element.182, f32[1,1536,64]{1,2,0:T(8,128)S(1)} %get-tuple-element.196, f32[1536]{0:T(1024)S(1)} %get-tuple-element.183, pred[]{:T(512)S(6)} %compare.14, ...), kind=kOutput, calls=%fused_computation.6.clone.1 | convolution fusion | flops 206340096 | bytes 7221253 | tf_op jit(solution)/shard_map/while/body/eval_jaxpr/dot_general | solution.py:108
  93.5 1.1 fusion.65
  94.6 2.2 %fusion.67 = f32[1,1536,64]{1,2,0:T(8,128)S(1)} fusion(f32[1024,1536]{1,0:T(8,128)S(1)} %get-tuple-element.181, f32[1536]{0:T(1024)S(1)} %get-tuple-element.182, f32[1,1536,64]{1,2,0:T(8,128)S(1)} %get-tuple-element.196, f32[1536]{0:T(1024)S(1)} %get-tuple-element.183, pred[]{:T(512)S(6)} %compare.14, ...), kind=kOutput, calls=%fused_computation.6.clone.1 | convolution fusion | flops 206340096 | bytes 7221253 | tf_op jit(solution)/shard_map/while/body/eval_jaxpr/dot_general | solution.py:108
  97.9 1.1 fusion.65
  99.0 2.2 %fusion.67 = f32[1,1536,64]{1,2,0:T(8,128)S(1)} fusion(f32[1024,1536]{1,0:T(8,128)S(1)} %get-tuple-element.181, f32[1536]{0:T(1024)S(1)} %get-tuple-element.182, f32[1,1536,64]{1,2,0:T(8,128)S(1)} %get-tuple-element.196, f32[1536]{0:T(1024)S(1)} %get-tuple-element.183, pred[]{:T(512)S(6)} %compare.14, ...), kind=kOutput, calls=%fused_computation.6.clone.1 | convolution fusion | flops 206340096 | bytes 7221253 | tf_op jit(solution)/shard_map/while/body/eval_jaxpr/dot_general | solution.py:108
  102.3 1.1 fusion.65
  103.4 2.2 %fusion.67 = f32[1,1536,64]{1,2,0:T(8,128)S(1)} fusion(f32[1024,1536]{1,0:T(8,128)S(1)} %get-tuple-element.181, f32[1536]{0:T(1024)S(1)} %get-tuple-element.182, f32[1,1536,64]{1,2,0:T(8,128)S(1)} %get-tuple-element.196, f32[1536]{0:T(1024)S(1)} %get-tuple-element.183, pred[]{:T(512)S(6)} %compare.14, ...), kind=kOutput, calls=%fused_computation.6.clone.1 | convolution fusion | flops 206340096 | bytes 7221253 | tf_op jit(solution)/shard_map/while/body/eval_jaxpr/dot_general | solution.py:108
  106.7 1.1 fusion.65
  107.8 2.2 %fusion.67 = f32[1,1536,64]{1,2,0:T(8,128)S(1)} fusion(f32[1024,1536]{1,0:T(8,128)S(1)} %get-tuple-element.181, f32[1536]{0:T(1024)S(1)} %get-tuple-element.182, f32[1,1536,64]{1,2,0:T(8,128)S(1)} %get-tuple-element.196, f32[1536]{0:T(1024)S(1)} %get-tuple-element.183, pred[]{:T(512)S(6)} %compare.14, ...), kind=kOutput, calls=%fused_computation.6.clone.1 | convolution fusion | flops 206340096 | bytes 7221253 | tf_op jit(solution)/shard_map/while/body/eval_jaxpr/dot_general | solution.py:108
  111.1 1.1 fusion.65
  112.2 2.2 %fusion.67 = f32[1,1536,64]{1,2,0:T(8,128)S(1)} fusion(f32[1024,1536]{1,0:T(8,128)S(1)} %get-tuple-element.181, f32[1536]{0:T(1024)S(1)} %get-tuple-element.182, f32[1,1536,64]{1,2,0:T(8,128)S(1)} %get-tuple-element.196, f32[1536]{0:T(1024)S(1)} %get-tuple-element.183, pred[]{:T(512)S(6)} %compare.14, ...), kind=kOutput, calls=%fused_computation.6.clone.1 | convolution fusion | flops 206340096 | bytes 7221253 | tf_op jit(solution)/shard_map/while/body/eval_jaxpr/dot_general | solution.py:108
  115.5 1.1 fusion.65
  116.6 2.2 %fusion.67 = f32[1,1536,64]{1,2,0:T(8,128)S(1)} fusion(f32[1024,1536]{1,0:T(8,128)S(1)} %get-tuple-element.181, f32[1536]{0:T(1024)S(1)} %get-tuple-element.182, f32[1,1536,64]{1,2,0:T(8,128)S(1)} %get-tuple-element.196, f32[1536]{0:T(1024)S(1)} %get-tuple-element.183, pred[]{:T(512)S(6)} %compare.14, ...), kind=kOutput, calls=%fused_computation.6.clone.1 | convolution fusion | flops 206340096 | bytes 7221253 | tf_op jit(solution)/shard_map/while/body/eval_jaxpr/dot_general | solution.py:108
  119.9 1.1 fusion.65
  121.0 2.2 %fusion.67 = f32[1,1536,64]{1,2,0:T(8,128)S(1)} fusion(f32[1024,1536]{1,0:T(8,128)S(1)} %get-tuple-element.181, f32[1536]{0:T(1024)S(1)} %get-tuple-element.182, f32[1,1536,64]{1,2,0:T(8,128)S(1)} %get-tuple-element.196, f32[1536]{0:T(1024)S(1)} %get-tuple-element.183, pred[]{:T(512)S(6)} %compare.14, ...), kind=kOutput, calls=%fused_computation.6.clone.1 | convolution fusion | flops 206340096 | bytes 7221253 | tf_op jit(solution)/shard_map/while/body/eval_jaxpr/dot_general | solution.py:108
  125.3 2.2 %fusion.67 = f32[1,1536,64]{1,2,0:T(8,128)S(1)} fusion(f32[1024,1536]{1,0:T(8,128)S(1)} %get-tuple-element.181, f32[1536]{0:T(1024)S(1)} %get-tuple-element.182, f32[1,1536,64]{1,2,0:T(8,128)S(1)} %get-tuple-element.196, f32[1536]{0:T(1024)S(1)} %get-tuple-element.183, pred[]{:T(512)S(6)} %compare.14, ...), kind=kOutput, calls=%fused_computation.6.clone.1 | convolution fusion | flops 206340096 | bytes 7221253 | tf_op jit(solution)/shard_map/while/body/eval_jaxpr/dot_general | solution.py:108
  128.6 1.1 fusion.65
  129.7 2.2 %fusion.67 = f32[1,1536,64]{1,2,0:T(8,128)S(1)} fusion(f32[1024,1536]{1,0:T(8,128)S(1)} %get-tuple-element.181, f32[1536]{0:T(1024)S(1)} %get-tuple-element.182, f32[1,1536,64]{1,2,0:T(8,128)S(1)} %get-tuple-element.196, f32[1536]{0:T(1024)S(1)} %get-tuple-element.183, pred[]{:T(512)S(6)} %compare.14, ...), kind=kOutput, calls=%fused_computation.6.clone.1 | convolution fusion | flops 206340096 | bytes 7221253 | tf_op jit(solution)/shard_map/while/body/eval_jaxpr/dot_general | solution.py:108
  134.1 2.2 %fusion.67 = f32[1,1536,64]{1,2,0:T(8,128)S(1)} fusion(f32[1024,1536]{1,0:T(8,128)S(1)} %get-tuple-element.181, f32[1536]{0:T(1024)S(1)} %get-tuple-element.182, f32[1,1536,64]{1,2,0:T(8,128)S(1)} %get-tuple-element.196, f32[1536]{0:T(1024)S(1)} %get-tuple-element.183, pred[]{:T(512)S(6)} %compare.14, ...), kind=kOutput, calls=%fused_computation.6.clone.1 | convolution fusion | flops 206340096 | bytes 7221253 | tf_op jit(solution)/shard_map/while/body/eval_jaxpr/dot_general | solution.py:108
  137.4 1.1 fusion.65
  138.5 2.2 %fusion.67 = f32[1,1536,64]{1,2,0:T(8,128)S(1)} fusion(f32[1024,1536]{1,0:T(8,128)S(1)} %get-tuple-element.181, f32[1536]{0:T(1024)S(1)} %get-tuple-element.182, f32[1,1536,64]{1,2,0:T(8,128)S(1)} %get-tuple-element.196, f32[1536]{0:T(1024)S(1)} %get-tuple-element.183, pred[]{:T(512)S(6)} %compare.14, ...), kind=kOutput, calls=%fused_computation.6.clone.1 | convolution fusion | flops 206340096 | bytes 7221253 | tf_op jit(solution)/shard_map/while/body/eval_jaxpr/dot_general | solution.py:108
  141.3 1.7 convolution_convert_fusion
  144.0 24.2 %reduce-scatter.2.cloned.1.call-done = bf16[96,2048]{1,0:T(8,128)(2,1)} async-done(((bf16[384,2048]{1,0:T(8,128)(2,1)}), bf16[96,2048]{1,0:T(8,128)(2,1)}) %reduce-scatter.2.cloned.1.call-update) | async-done | bytes 393232 | tf_op jit(solution)/shard_map/reduce_scatter | solution.py:157
  (93 shorter events, 21.4 us)
Async XLA Ops:
  7.2 134.1 %copy-start = (bf16[256,2048]{1,0:T(8,128)(2,1)S(1)}, bf16[256,2048]{1,0:T(8,128)(2,1)}, u32[]{:S(2)}) copy-start(bf16[256,2048]{1,0:T(8,128)(2,1)} %param.13) | copy-start | bytes 3145732
  9.6 4.6 %copy-start.4 = (bf16[1,64]{1,0:T(2,128)(2,1)S(1)}, bf16[1,64]{1,0:T(2,128)(2,1)}, u32[]{:S(2)}) copy-start(bf16[1,64]{1,0:T(2,128)(2,1)} %param.15) | copy-start | bytes 388
  9.6 25.3 %copy-start.1 = (bf16[2048,64]{0,1:T(8,128)(2,1)S(1)}, bf16[2048,64]{0,1:T(8,128)(2,1)}, u32[]{:S(2)}) copy-start(bf16[2048,64]{0,1:T(8,128)(2,1)} %param.12) | copy-start | bytes 786436
  9.6 25.2 %all-to-all-start = ((bf16[4,96,2048]{2,1,0:T(8,128)(2,1)}), bf16[4,96,2048]{2,1,0:T(8,128)(2,1)S(1)}, u32[]{:S(2)}, u32[]{:S(2)}) async-start(bf16[4,96,2048]{2,1,0:T(8,128)(2,1)} %broadcast_in_dim.11), calls=%async_computation | async-start | bytes 3145728 | tf_op jit(solution)/shard_map/all_to_all | solution.py:19
  14.1 21.3 %copy-start.2 = (bf16[2048,64]{0,1:T(8,128)(2,1)S(1)}, bf16[2048,64]{0,1:T(8,128)(2,1)}, u32[]{:S(2)}) copy-start(bf16[2048,64]{0,1:T(8,128)(2,1)} %param.11) | copy-start | bytes 786436
  14.1 70.3 %all-gather.2.cloned.1.call-start = ((), (), s32[]{:S(2)}) async-start(), calls=%async_computation.2 | async-start | bytes 3244032 | tf_op jit(solution)/shard_map/all_gather | solution.py:31
  35.5 1.8 %copy-start.3 = (bf16[4,64]{1,0:T(4,128)(2,1)S(1)}, bf16[4,64]{1,0:T(4,128)(2,1)}, u32[]{:S(2)}) copy-start(bf16[4,64]{1,0:T(4,128)(2,1)} %param.14) | copy-start | bytes 1540
  37.1 131.1 %reduce-scatter.2.cloned.1.call-start = ((), (), s32[]{:S(2)}) async-start(), calls=%async_computation.3 | async-start | bytes 1966080 | tf_op jit(solution)/shard_map/reduce_scatter | solution.py:157
Sparse Core Ops, SparseCore 0:
  37.3 47.1 all-gather.1
  143.2 24.9 reduce-scatter.1
where the time goes:
time: 176 us; the launch traced here: 175 us
  waiting for transfers between devices  88.1 us (50%)
  matrix products  43.3 us (25%)
  other arithmetic  15.8 us (9%)
  between operations  14.3 us (8%)
  local copies, waits for them, and re-layouts  8.47 us (5%)
  starting transfers between devices  4.58 us (3%)
    all_gather x1, waiting for transfers between devices, side_by_side(): out = lax.all_gather(both, axis, axis=dim, tiled=True)  43.2 us
    dot_general x12, matrix products, inner(): lax.dot_general(expo.astype(jnp.bfloat16), value_block, (((2,), (0,)), ((...  26 us
    reduce_scatter x1, waiting for transfers between devices, body(): lax.psum_scatter(jnp.dot(attended, out_weight, preferred_element_type=jnp...  24.2 us
    all_to_all x1, waiting for transfers between devices, copy_for_each(): lax.all_to_all(jnp.broadcast_to(array[None], (count, *array.shape)), axis...  20.7 us
    reduce_sum x12, other arithmetic, inner(): total = total * factor + jnp.sum(expo, axis=-1)  12.8 us
    dot_general x12, matrix products, inner(): lax.dot_general(grouped, key_block, (((2,), (2,)), ((0,), (1,))), preferr...  12.4 us
    all_to_all x1, starting transfers between devices, copy_for_each(): lax.all_to_all(jnp.broadcast_to(array[None], (count, *array.shape)), axis...  4.54 us
  transfers between devices with their start and end apart: 3, of which 3 were waited for; matrix products, arithmetic and copies ran while one was open for 3% of the time, Pallas kernels for 0%

commit v1 on v0

--- a/solution.py
+++ b/solution.py
@@ -16,9 +16,7 @@
 
 def copy_for_each(array, axis):
     count = lax.axis_size(axis)
-    return lax.all_to_all(
-        jnp.broadcast_to(array[None], (count, *array.shape)), axis, 0, 0, tiled=True
-    )
+    return lax.all_gather(array, axis, axis=0)
 
 
 def collect(array, axis, dim):

time: 176 us -> 181 us (1.028)
  waiting for transfers between devices: 88.1 us -> 97.5 us
  starting transfers between devices: 4.58 us -> 0.12 us
  matrix products: 43.3 us -> 46.3 us
  local copies, waits for them, and re-layouts: 8.47 us -> 6.04 us
    all_gather x0 -> x1, waiting for transfers between devices: none -> 29.9 us  [copy_for_each(): return lax.all_gather(array, axis, axis=0)]
    all_to_all x1 -> x0, waiting for transfers between devices: 20.7 us -> none  [copy_for_each(): lax.all_to_all(jnp.broadcast_to(array[None], (count, *array.shape)), axis...]
    all_to_all x1 -> x0, starting transfers between devices: 4.54 us -> none  [copy_for_each(): lax.all_to_all(jnp.broadcast_to(array[None], (count, *array.shape)), axis...]
    dot_general x3, matrix products: 3.2 us -> 6.17 us  [body(): jnp.dot(piece, weight, preferred_element_type=jnp.float32)]
    broadcast_in_dim x1 -> x0, local copies, waits for them, and re-layouts: 2.43 us -> none  [copy_for_each(): jnp.broadcast_to(array[None], (count, *array.shape))]
where the time goes in v1:
time: 181 us
  waiting for transfers between devices  97.5 us (54%)
  matrix products  46.3 us (26%)
  other arithmetic  16.4 us (9%)
  between operations  14 us (8%)
  local copies, waits for them, and re-layouts  6.04 us (3%)
    all_gather x1, waiting for transfers between devices, side_by_side(): out = lax.all_gather(both, axis, axis=dim, tiled=True)  42.7 us
    all_gather x1, waiting for transfers between devices, copy_for_each(): return lax.all_gather(array, axis, axis=0)  29.9 us
    dot_general x12, matrix products, inner(): lax.dot_general(expo.astype(jnp.bfloat16), value_block, (((2,), (0,)), ((...  26 us
    reduce_scatter x1, waiting for transfers between devices, body(): lax.psum_scatter(jnp.dot(attended, out_weight, preferred_element_type=jnp...  24.2 us
    reduce_sum x12, other arithmetic, inner(): total = total * factor + jnp.sum(expo, axis=-1)  12.8 us
    dot_general x12, matrix products, inner(): lax.dot_general(grouped, key_block, (((2,), (2,)), ((0,), (1,))), preferr...  12.4 us
    dot_general x3, matrix products, body(): jnp.dot(piece, weight, preferred_element_type=jnp.float32)  6.17 us
  transfers between devices with their start and end apart: 3, of which 3 were waited for; matrix products, arithmetic and copies ran while one was open for 3% of the time, Pallas kernels for 0%

profile of v1, /device:TPU:0, one launch (start us, length us, event | category | flops | bytes accessed | tf_op | source)
XLA Modules:
  0.0 180.9 jit_solution(1883148416852422429)
XLA Ops:
  8.7 29.9 %all-gather.6.cloned.1.call-done = bf16[384,2048]{1,0:T(8,128)(2,1)} async-done(((bf16[96,2048]{1,0:T(8,128)(2,1)}), bf16[384,2048]{1,0:T(8,128)(2,1)}) %all-gather.6.cloned.1.call-update) | async-done | bytes 1572880 | tf_op jit(solution)/shard_map/all_gather | solution.py:19
  38.6 2.2 %multiply_reduce_fusion.1 = (f32[384]{0:T(512)S(1)}, f32[384,64]{0,1:T(8,128)S(1)}) fusion(bf16[384,2048]{1,0:T(8,128)(2,1)} %all-gather.6.cloned.1.call-done, bf16[2048,64]{0,1:T(8,128)(2,1)} %param.11), kind=kOutput, calls=%fused_computation.44 | convolution fusion | flops 100761216 | bytes 1934848 | tf_op jit(solution)/shard_map/dot_general | solution.py:138
  41.1 2.0 %fusion.23 = bf16[384,1,64]{0,2,1:T(8,128)(2,1)S(1)} fusion(bf16[384,2048]{1,0:T(8,128)(2,1)} %all-gather.6.cloned.1.call-done, bf16[2048,64]{0,1:T(8,128)(2,1)} %param.12), kind=kOutput, calls=%fused_computation.31 | convolution fusion | flops 100687872 | bytes 1884160 | tf_op jit(solution)/shard_map/dot_general | solution.py:138
  44.2 2.0 %fusion.24 = (f32[384,4]{0,1:T(4,128)S(1)}, bf16[384,256]{0,1:T(8,128)(2,1)S(1)}) fusion(bf16[384,2048]{1,0:T(8,128)(2,1)S(1)} %copy-done.1, bf16[2048,256]{1,0:T(8,128)(2,1)} %param.10), kind=kOutput, calls=%fused_computation.34 | convolution fusion | flops 403044864 | bytes 2824192 | tf_op jit(solution)/shard_map/dot_general | solution.py:138
  47.9 42.7 %all-gather.4.cloned.1.call-done = bf16[12288,2,64]{0,2,1:T(8,128)(2,1)} async-done(((bf16[384,2,64]{0,2,1:T(8,128)(2,1)}), bf16[12288,2,64]{0,2,1:T(8,128)(2,1)}) %all-gather.4.cloned.1.call-update) | async-done | bytes 3145744 | tf_op jit(solution)/shard_map/all_gather | solution.py:29
  90.6 2.2 %fusion.47 = (bf16[12288,1,64]{0,2,1:T(8,128)(2,1)S(1)}, bf16[12288,1,64]{0,2,1:T(8,128)(2,1)S(1)}) fusion(bf16[12288,2,64]{0,2,1:T(8,128)(2,1)} %all-gather.4.cloned.1.call-done), kind=kLoop, calls=%fused_computation.86 | loop fusion | bytes 6291456 | tf_op jit(solution)/shard_map/split | solution.py:30
  92.9 1.3 copy.27
  94.2 52.6 %while.15 = (s32[]{:T(128)}, f32[1,1536]{1,0:T(1,128)S(1)}, f32[1,1536]{1,0:T(1,128)S(1)}, f32[1,1536,64]{1,2,0:T(8,128)S(1)}, bf16[12,1024,1,64]{1,3,2,0:T(8,12...) while((s32[]{:T(128)}, f32[1,1536]{1,0:T(1,128)S(1)}, ...), condition=%wide.region_5.6_spmd.clone, body=%wide.region_2.5_spmd.clone.sunk | while | flops 415540224 | bytes 20420728 | solution.py:115
  95.3 1.1 fusion.65
  96.4 2.2 %fusion.67 = f32[1,1536,64]{1,2,0:T(8,128)S(1)} fusion(f32[1024,1536]{1,0:T(8,128)S(1)} %get-tuple-element.181, f32[1536]{0:T(1024)S(1)} %get-tuple-element.182, f32[1,1536,64]{1,2,0:T(8,128)S(1)} %get-tuple-element.196, f32[1536]{0:T(1024)S(1)} %get-tuple-element.183, pred[]{:T(512)S(6)} %compare.14, ...), kind=kOutput, calls=%fused_computation.6.clone.1 | convolution fusion | flops 206340096 | bytes 7221253 | tf_op jit(solution)/shard_map/while/body/eval_jaxpr/dot_general | solution.py:106
  99.7 1.1 fusion.65
  100.8 2.2 %fusion.67 = f32[1,1536,64]{1,2,0:T(8,128)S(1)} fusion(f32[1024,1536]{1,0:T(8,128)S(1)} %get-tuple-element.181, f32[1536]{0:T(1024)S(1)} %get-tuple-element.182, f32[1,1536,64]{1,2,0:T(8,128)S(1)} %get-tuple-element.196, f32[1536]{0:T(1024)S(1)} %get-tuple-element.183, pred[]{:T(512)S(6)} %compare.14, ...), kind=kOutput, calls=%fused_computation.6.clone.1 | convolution fusion | flops 206340096 | bytes 7221253 | tf_op jit(solution)/shard_map/while/body/eval_jaxpr/dot_general | solution.py:106
  104.1 1.1 fusion.65
  105.2 2.2 %fusion.67 = f32[1,1536,64]{1,2,0:T(8,128)S(1)} fusion(f32[1024,1536]{1,0:T(8,128)S(1)} %get-tuple-element.181, f32[1536]{0:T(1024)S(1)} %get-tuple-element.182, f32[1,1536,64]{1,2,0:T(8,128)S(1)} %get-tuple-element.196, f32[1536]{0:T(1024)S(1)} %get-tuple-element.183, pred[]{:T(512)S(6)} %compare.14, ...), kind=kOutput, calls=%fused_computation.6.clone.1 | convolution fusion | flops 206340096 | bytes 7221253 | tf_op jit(solution)/shard_map/while/body/eval_jaxpr/dot_general | solution.py:106
  108.5 1.1 fusion.65
  109.6 2.2 %fusion.67 = f32[1,1536,64]{1,2,0:T(8,128)S(1)} fusion(f32[1024,1536]{1,0:T(8,128)S(1)} %get-tuple-element.181, f32[1536]{0:T(1024)S(1)} %get-tuple-element.182, f32[1,1536,64]{1,2,0:T(8,128)S(1)} %get-tuple-element.196, f32[1536]{0:T(1024)S(1)} %get-tuple-element.183, pred[]{:T(512)S(6)} %compare.14, ...), kind=kOutput, calls=%fused_computation.6.clone.1 | convolution fusion | flops 206340096 | bytes 7221253 | tf_op jit(solution)/shard_map/while/body/eval_jaxpr/dot_general | solution.py:106
  112.8 1.1 fusion.65
  114.0 2.2 %fusion.67 = f32[1,1536,64]{1,2,0:T(8,128)S(1)} fusion(f32[1024,1536]{1,0:T(8,128)S(1)} %get-tuple-element.181, f32[1536]{0:T(1024)S(1)} %get-tuple-element.182, f32[1,1536,64]{1,2,0:T(8,128)S(1)} %get-tuple-element.196, f32[1536]{0:T(1024)S(1)} %get-tuple-element.183, pred[]{:T(512)S(6)} %compare.14, ...), kind=kOutput, calls=%fused_computation.6.clone.1 | convolution fusion | flops 206340096 | bytes 7221253 | tf_op jit(solution)/shard_map/while/body/eval_jaxpr/dot_general | solution.py:106
  117.2 1.1 fusion.65
  118.3 2.2 %fusion.67 = f32[1,1536,64]{1,2,0:T(8,128)S(1)} fusion(f32[1024,1536]{1,0:T(8,128)S(1)} %get-tuple-element.181, f32[1536]{0:T(1024)S(1)} %get-tuple-element.182, f32[1,1536,64]{1,2,0:T(8,128)S(1)} %get-tuple-element.196, f32[1536]{0:T(1024)S(1)} %get-tuple-element.183, pred[]{:T(512)S(6)} %compare.14, ...), kind=kOutput, calls=%fused_computation.6.clone.1 | convolution fusion | flops 206340096 | bytes 7221253 | tf_op jit(solution)/shard_map/while/body/eval_jaxpr/dot_general | solution.py:106
  121.6 1.1 fusion.65
  122.7 2.2 %fusion.67 = f32[1,1536,64]{1,2,0:T(8,128)S(1)} fusion(f32[1024,1536]{1,0:T(8,128)S(1)} %get-tuple-element.181, f32[1536]{0:T(1024)S(1)} %get-tuple-element.182, f32[1,1536,64]{1,2,0:T(8,128)S(1)} %get-tuple-element.196, f32[1536]{0:T(1024)S(1)} %get-tuple-element.183, pred[]{:T(512)S(6)} %compare.14, ...), kind=kOutput, calls=%fused_computation.6.clone.1 | convolution fusion | flops 206340096 | bytes 7221253 | tf_op jit(solution)/shard_map/while/body/eval_jaxpr/dot_general | solution.py:106
  126.0 1.1 fusion.65
  127.1 2.2 %fusion.67 = f32[1,1536,64]{1,2,0:T(8,128)S(1)} fusion(f32[1024,1536]{1,0:T(8,128)S(1)} %get-tuple-element.181, f32[1536]{0:T(1024)S(1)} %get-tuple-element.182, f32[1,1536,64]{1,2,0:T(8,128)S(1)} %get-tuple-element.196, f32[1536]{0:T(1024)S(1)} %get-tuple-element.183, pred[]{:T(512)S(6)} %compare.14, ...), kind=kOutput, calls=%fused_computation.6.clone.1 | convolution fusion | flops 206340096 | bytes 7221253 | tf_op jit(solution)/shard_map/while/body/eval_jaxpr/dot_general | solution.py:106
  130.4 1.1 fusion.65
  131.5 2.2 %fusion.67 = f32[1,1536,64]{1,2,0:T(8,128)S(1)} fusion(f32[1024,1536]{1,0:T(8,128)S(1)} %get-tuple-element.181, f32[1536]{0:T(1024)S(1)} %get-tuple-element.182, f32[1,1536,64]{1,2,0:T(8,128)S(1)} %get-tuple-element.196, f32[1536]{0:T(1024)S(1)} %get-tuple-element.183, pred[]{:T(512)S(6)} %compare.14, ...), kind=kOutput, calls=%fused_computation.6.clone.1 | convolution fusion | flops 206340096 | bytes 7221253 | tf_op jit(solution)/shard_map/while/body/eval_jaxpr/dot_general | solution.py:106
  134.8 1.1 fusion.65
  135.9 2.2 %fusion.67 = f32[1,1536,64]{1,2,0:T(8,128)S(1)} fusion(f32[1024,1536]{1,0:T(8,128)S(1)} %get-tuple-element.181, f32[1536]{0:T(1024)S(1)} %get-tuple-element.182, f32[1,1536,64]{1,2,0:T(8,128)S(1)} %get-tuple-element.196, f32[1536]{0:T(1024)S(1)} %get-tuple-element.183, pred[]{:T(512)S(6)} %compare.14, ...), kind=kOutput, calls=%fused_computation.6.clone.1 | convolution fusion | flops 206340096 | bytes 7221253 | tf_op jit(solution)/shard_map/while/body/eval_jaxpr/dot_general | solution.py:106
  140.3 2.2 %fusion.67 = f32[1,1536,64]{1,2,0:T(8,128)S(1)} fusion(f32[1024,1536]{1,0:T(8,128)S(1)} %get-tuple-element.181, f32[1536]{0:T(1024)S(1)} %get-tuple-element.182, f32[1,1536,64]{1,2,0:T(8,128)S(1)} %get-tuple-element.196, f32[1536]{0:T(1024)S(1)} %get-tuple-element.183, pred[]{:T(512)S(6)} %compare.14, ...), kind=kOutput, calls=%fused_computation.6.clone.1 | convolution fusion | flops 206340096 | bytes 7221253 | tf_op jit(solution)/shard_map/while/body/eval_jaxpr/dot_general | solution.py:106
  144.7 2.2 %fusion.67 = f32[1,1536,64]{1,2,0:T(8,128)S(1)} fusion(f32[1024,1536]{1,0:T(8,128)S(1)} %get-tuple-element.181, f32[1536]{0:T(1024)S(1)} %get-tuple-element.182, f32[1,1536,64]{1,2,0:T(8,128)S(1)} %get-tuple-element.196, f32[1536]{0:T(1024)S(1)} %get-tuple-element.183, pred[]{:T(512)S(6)} %compare.14, ...), kind=kOutput, calls=%fused_computation.6.clone.1 | convolution fusion | flops 206340096 | bytes 7221253 | tf_op jit(solution)/shard_map/while/body/eval_jaxpr/dot_general | solution.py:106
  147.5 1.7 convolution_convert_fusion
  150.1 24.2 %reduce-scatter.2.cloned.1.call-done = bf16[96,2048]{1,0:T(8,128)(2,1)} async-done(((bf16[384,2048]{1,0:T(8,128)(2,1)}), bf16[96,2048]{1,0:T(8,128)(2,1)}) %reduce-scatter.2.cloned.1.call-update) | async-done | bytes 393232 | tf_op jit(solution)/shard_map/reduce_scatter | solution.py:155
  (89 shorter events, 21.6 us)
Async XLA Ops:
  7.2 140.3 %copy-start = (bf16[256,2048]{1,0:T(8,128)(2,1)S(1)}, bf16[256,2048]{1,0:T(8,128)(2,1)}, u32[]{:S(2)}) copy-start(bf16[256,2048]{1,0:T(8,128)(2,1)} %param.13) | copy-start | bytes 3145732
  7.2 36.7 %copy-start.2 = (bf16[4,64]{1,0:T(4,128)(2,1)S(1)}, bf16[4,64]{1,0:T(4,128)(2,1)}, u32[]{:S(2)}) copy-start(bf16[4,64]{1,0:T(4,128)(2,1)} %param.14) | copy-start | bytes 1540
  7.2 31.4 %all-gather.6.cloned.1.call-start = ((), (), s32[]{:S(2)}) async-start(), calls=%async_computation.3 | async-start | bytes 1966080 | tf_op jit(solution)/shard_map/all_gather | solution.py:19
  7.9 82.7 %all-gather.4.cloned.1.call-start = ((), (), s32[]{:S(2)}) async-start(), calls=%async_computation.1 | async-start | bytes 3244032 | tf_op jit(solution)/shard_map/all_gather | solution.py:29
  38.6 5.6 %copy-start.1 = (bf16[384,2048]{1,0:T(8,128)(2,1)S(1)}, bf16[384,2048]{1,0:T(8,128)(2,1)}, u32[]{:S(2)}) copy-start(bf16[384,2048]{1,0:T(8,128)(2,1)} %all-gather.6.cloned.1.call-done) | copy-start | bytes 4718596
  43.8 130.5 %reduce-scatter.2.cloned.1.call-start = ((), (), s32[]{:S(2)}) async-start(), calls=%async_computation.2 | async-start | bytes 1966080 | tf_op jit(solution)/shard_map/reduce_scatter | solution.py:155
Sparse Core Ops, SparseCore 0:
  9.7 28.9 all-gather.5
  44.0 46.5 all-gather.3
  149.3 24.9 reduce-scatter.1
